TPU v7x, 512 devices: a whole 4x8x8 slice. The times are simulated.
512 devices in a mesh: sp: 64 (over z, y), tp: 8 (over x, core).
Axes of the slice: x: 4, y: 8, z: 8, core: 2. Of those that a mesh axis runs over, the one named last changes fastest.
Arguments:
- queries: bfloat16 [16384, 512], P('sp', 'tp'), may hold values from -8 to 8
- keys: bfloat16 [16384, 512], P('sp', 'tp'), may hold values from -8 to 8
- values: bfloat16 [16384, 512], P('sp', 'tp'), may hold values from -6 to 6
- score_shift: float32 [8], P('tp'), may hold values from 3 to 20
- resid: bfloat16 [16384, 2048], P(('sp', 'tp')), may hold values from -6 to 6
- w_out: bfloat16 [512, 2048], replicated, may hold values from -0.25 to 0.25
- gain_mix: float32 [2048], replicated, may hold values from 0.1 to 1.9
- gain_pre: float32 [2048], replicated, may hold values from 0.1 to 1.9
- w_gate: bfloat16 [2048, 5632], P('sp', 'tp'), may hold values from -0.125 to 0.125
- w_up: bfloat16 [2048, 5632], P('sp', 'tp'), may hold values from -0.125 to 0.125
- conv_gate: float32 [3, 5632], P(None, 'tp'), may hold values from -3 to 3
- conv_up: float32 [3, 5632], P(None, 'tp'), may hold values from -3 to 3
- w_down: bfloat16 [5632, 2048], P('tp', 'sp'), may hold values from -0.078125 to 0.078125
- gain_post: float32 [2048], replicated, may hold values from 0.1 to 1.9
Outputs:
- result: bfloat16 [16384, 2048], P(('sp', 'tp'))
All inputs are finite; a program needn't handle non-finite values.
Results may differ from a plain program's by a relative error of at most 0.017.
Values may be sent and summed in bfloat16 or wider, within the bound.
A program may use at most 64 MiB of HBM per device.

v0:
```python
import jax
import jax.numpy as jnp
from jax import lax
from jax.sharding import PartitionSpec as P

HEAD_DIM = 64
KERNEL = 3


def side_by_side(arrays, axis, dim, along):
    widths = [a.shape[along] for a in arrays]
    both = jnp.concatenate(arrays, axis=along)
    out = lax.all_gather(both, axis, axis=dim, tiled=True)
    return tuple(jnp.split(out, [sum(widths[:k]) for k in range(1, len(widths))], axis=along))


def laid_out(parts, dim):
    parts = jnp.moveaxis(parts, 0, dim)
    lengths = parts.shape
    return parts.reshape(*lengths[:dim], lengths[dim] * lengths[dim + 1], *lengths[dim + 2 :])


def from_everyone(x, axis):
    length = lax.axis_size(axis)
    return lax.all_to_all(jnp.broadcast_to(x[None], (length, *x.shape)), axis, 0, 0, tiled=True)


def gathered_copies(x, axis, dim):
    return laid_out(from_everyone(x, axis), dim)


def from_behind(x, axis, by):
    length = lax.axis_size(axis)
    pairs = [(i, i + by) for i in range(length) if 0 <= i + by < length]
    return lax.ppermute(x, axis, pairs)


def split_up(x, dim, length):
    before, after = (x.shape[:dim], x.shape[dim + 1 :])
    return jnp.moveaxis(x.reshape(*before, length, -1, *after), dim, 0)


def sum_at_owner(x, axis, dim):
    parts = split_up(x, dim, lax.axis_size(axis))
    arrived = lax.all_to_all(parts, axis, split_axis=0, concat_axis=0, tiled=True)
    return arrived.astype(jnp.float32).sum(axis=0)


def rms_scale(values_in):
    return values_in * lax.rsqrt(jnp.mean(values_in * values_in, axis=-1, keepdims=True) + 1e-06)


def collect_weights(w_gate, w_up, w_down):
    gate_whole, up_whole = side_by_side((w_gate, w_up), "sp", 0, 1)
    down_whole = lax.all_gather(w_down, "sp", axis=1, tiled=True)
    return (gate_whole, up_whole, down_whole)


def stick_attention(queries, key_whole, value_whole, score_shift):
    tok_rows = queries.shape[0]
    local_heads = queries.shape[1] // HEAD_DIM
    total = key_whole.shape[0]
    shards = total // tok_rows
    group = max(
        (
            factor
            for factor in range(1, shards + 1)
            if shards % factor == 0 and factor * tok_rows <= max(2048, tok_rows)
        )
    )
    span = group * tok_rows
    offset = lax.axis_index("sp") * tok_rows
    query_heads = queries.reshape(tok_rows, local_heads, HEAD_DIM)
    key_heads = key_whole.reshape(total, local_heads, HEAD_DIM)
    value_heads = value_whole.reshape(total, local_heads, HEAD_DIM)
    query_pos = offset + jnp.arange(tok_rows, dtype=jnp.int32)
    last_block = (offset + tok_rows - 1) // span

    def visit(turn, carry):
        accum, tail = carry
        block_start = (last_block - turn) * span
        key_block = lax.dynamic_slice_in_dim(key_heads, block_start, span, 0)
        value_block = lax.dynamic_slice_in_dim(value_heads, block_start, span, 0)
        scores = jnp.einsum(
            "qhd,khd->hqk", query_heads, key_block, preferred_element_type=jnp.float32
        )
        scores = scores * HEAD_DIM ** (-0.5) - score_shift[:, None, None]
        key_pos = block_start + jnp.arange(span, dtype=jnp.int32)
        causal = (key_pos[None, :] < query_pos[:, None])[None, :, :]
        log_keep = jnp.where(causal, -jax.nn.softplus(scores), 0.0)
        later = lax.cumsum(log_keep, axis=2, reverse=True) - log_keep
        weights = jnp.where(
            causal, jnp.exp(jax.nn.log_sigmoid(scores) + later + tail[:, :, None]), 0.0
        ).astype(jnp.bfloat16)
        accum = accum + jnp.einsum(
            "hqk,khd->hqd", weights, value_block, preferred_element_type=jnp.float32
        )
        return (accum, tail + jnp.sum(log_keep, axis=2))

    start_carry = (
        jnp.zeros((local_heads, tok_rows, HEAD_DIM), jnp.float32),
        jnp.zeros((local_heads, tok_rows), jnp.float32),
    )
    accum, _ = lax.fori_loop(0, last_block + 1, visit, start_carry)
    return accum.transpose(1, 0, 2).reshape(tok_rows, local_heads * HEAD_DIM).astype(jnp.bfloat16)


def local(
    queries,
    keys,
    values,
    score_shift,
    resid,
    w_out,
    gain_mix,
    gain_pre,
    w_gate,
    w_up,
    conv_gate,
    conv_up,
    w_down,
    gain_post,
):
    gate_whole, up_whole, down_whole = collect_weights(w_gate, w_up, w_down)
    key_whole, value_whole = side_by_side((keys, values), "sp", 0, 1)
    attended = stick_attention(queries, key_whole, value_whole, score_shift)
    head_rows = lax.all_to_all(attended, "tp", split_axis=0, concat_axis=1, tiled=True)
    mixed = jnp.dot(head_rows, w_out, preferred_element_type=jnp.float32).astype(jnp.bfloat16)
    middle = (resid.astype(jnp.float32) + gain_mix * rms_scale(mixed.astype(jnp.float32))).astype(
        jnp.bfloat16
    )
    normed = (gain_pre * rms_scale(middle.astype(jnp.float32))).astype(jnp.bfloat16)
    piece = gathered_copies(normed, "tp", 0)
    gate_part = jnp.dot(piece, gate_whole, preferred_element_type=jnp.float32).astype(jnp.bfloat16)
    up_part = jnp.dot(piece, up_whole, preferred_element_type=jnp.float32).astype(jnp.bfloat16)
    projected = jnp.concatenate([gate_part, up_part], axis=1)
    tok_rows = projected.shape[0]
    local_units = projected.shape[1] // 2
    edge = from_behind(projected[tok_rows - (KERNEL - 1) :], "sp", 1)
    extended = jnp.concatenate([edge, projected], axis=0).astype(jnp.float32)
    taps = jnp.concatenate([conv_gate, conv_up], axis=1)
    convolved = taps[0] * extended[0:tok_rows]
    for tap in range(1, KERNEL):
        convolved = convolved + taps[tap] * extended[tap : tap + tok_rows]
    hidden = (jax.nn.silu(convolved[:, :local_units]) * convolved[:, local_units:]).astype(
        jnp.bfloat16
    )
    summed = sum_at_owner(
        jnp.dot(hidden, down_whole, preferred_element_type=jnp.float32).astype(jnp.bfloat16),
        "tp",
        0,
    )
    ffn_out = summed.astype(jnp.bfloat16)
    return (middle.astype(jnp.float32) + gain_post * rms_scale(ffn_out.astype(jnp.float32))).astype(
        jnp.bfloat16
    )


def solution(mesh):
    in_specs = (
        P("sp", "tp"),
        P("sp", "tp"),
        P("sp", "tp"),
        P("tp"),
        P(("sp", "tp"), None),
        P(),
        P(),
        P(),
        P("sp", "tp"),
        P("sp", "tp"),
        P(None, "tp"),
        P(None, "tp"),
        P("tp", "sp"),
        P(),
    )
    out_specs = P(("sp", "tp"), None)
    return jax.shard_map(local, mesh=mesh, in_specs=in_specs, out_specs=out_specs, check_vma=False)
```

profile of v0, /device:TPU:448, one launch (start us, length us, event | category | flops | bytes accessed | tf_op | source)
XLA Modules:
  0.0 331.4 jit_solution(313989612567962187)
XLA Ops:
  6.5 1.6 pad_maximum_fusion.2
  8.2 1.5 pad_maximum_fusion.1
  9.8 0.7 all-gather.8.cloned.1.call-update
  10.5 88.7 %all-gather.4.cloned.1.call-done = bf16[16384,128]{0,1:T(8,128)(2,1)} async-done(((bf16[256,128]{0,1:T(8,128)(2,1)}), bf16[16384,128]{0,1:T(8,128)(2,1)}) %all-gather.4.cloned.1.call-update) | async-done | bytes 4194320 | tf_op jit(solution)/shard_map/all_gather | solution.py:13
  99.2 4.5 %slice_bitcast_fusion.2 = (bf16[16384,1,64]{0,2,1:T(8,128)(2,1)}, bf16[16384,1,64]{0,2,1:T(8,128)(2,1)}) fusion(bf16[16384,128]{0,1:T(8,128)(2,1)} %all-gather.4.cloned.1.call-done), kind=kLoop, calls=%fused_computation.39 | loop fusion | bytes 8388608 | tf_op jit(solution)/shard_map/reshape | solution.py:75
  103.8 146.1 %while.13 = (s32[]{:T(128)}, f32[1,256,64]{1,2,0:T(8,128)S(1)}, f32[1,256]{1,0:T(1,128)S(1)}, s32[]{:T(128)}, s32[]{:T(128)}, /*index=5*/bf16[16384,1,64]{0,2,1:...) while((s32[]{:T(128)}, f32[1,256,64]{1,2,0:T(8,128)S(1)}, ...), condition=%wide.region_4.5_spmd.clone, body=%wide.region_0.4_spmd.clone.sunk | while | flops 219236352 | bytes 19711708 | solution.py:104
  103.8 4.6 %fusion.62 = (f32[256]{0:T(256)S(1)}, f32[256,2048]{0,1:T(8,128)S(1)}, f32[256,2048]{0,1:T(8,128)}) fusion(s32[256]{0:T(256)S(1)} %iota_add_fusion.4, s32[2048]{0:T(1024)S(1)} %iota_add_fusion.5, f32[]{:T(128)} %bitcast.72, bf16[256,1,64]{0,2,1:T(8,128)(2,1)S(1)} %get-tuple-element.219, bf16[16384,1,64]{0,2,1:T(8,128)(2,1)} %get-tuple-element.218, ...), kind=kOutput, calls=%fused_computation.31.clone.1 | convolution fusion | flops 73400064 | bytes 4499972 | tf_op jit(solution)/shard_map/while/body/qhd,khd->hqk/dot_general | solution.py:84
  108.4 5.0 %fusion.63 = f32[1,256,16,128]{1,2,3,0:T(8,128)S(1)} fusion(f32[1,256,16,128]{1,3,2,0:T(8,128)S(1)} %bitcast.76), kind=kOutput, calls=%fused_computation.16.clone.1 | output fusion | flops 66584576 | bytes 4194304 | tf_op jit(solution)/shard_map/reduce-window
  113.4 2.6 copy.29
  116.1 4.6 %fusion.64 = bf16[256,2048]{0,1:T(8,128)(2,1)S(1)} fusion(f32[1,256,16,128]{1,3,2,0:T(8,128)} %copy.29, f32[256,2048]{0,1:T(8,128)} %get-tuple-element.181, f32[256]{0:T(256)S(1)} %bitcast.82, f32[256,16]{0,1:T(8,128)S(1)} %slice_bitcast_fusion.7, s32[256]{0:T(256)S(1)} %iota_add_fusion.4, s32[2048]{0:T(1024)S(1)} %iota_add_fusion.5), kind=kLoop, calls=%fused_computation.8.clone.1 | loop fusion | flops 12058624 | bytes 5269504 | tf_op jit(solution)/shard_map/while/body/convert_element_type | solution.py:94
  120.8 1.3 fusion.65
  122.1 4.6 %fusion.62 = (f32[256]{0:T(256)S(1)}, f32[256,2048]{0,1:T(8,128)S(1)}, f32[256,2048]{0,1:T(8,128)}) fusion(s32[256]{0:T(256)S(1)} %iota_add_fusion.4, s32[2048]{0:T(1024)S(1)} %iota_add_fusion.5, f32[]{:T(128)} %bitcast.72, bf16[256,1,64]{0,2,1:T(8,128)(2,1)S(1)} %get-tuple-element.219, bf16[16384,1,64]{0,2,1:T(8,128)(2,1)} %get-tuple-element.218, ...), kind=kOutput, calls=%fused_computation.31.clone.1 | convolution fusion | flops 73400064 | bytes 4499972 | tf_op jit(solution)/shard_map/while/body/qhd,khd->hqk/dot_general | solution.py:84
  126.6 5.0 %fusion.63 = f32[1,256,16,128]{1,2,3,0:T(8,128)S(1)} fusion(f32[1,256,16,128]{1,3,2,0:T(8,128)S(1)} %bitcast.76), kind=kOutput, calls=%fused_computation.16.clone.1 | output fusion | flops 66584576 | bytes 4194304 | tf_op jit(solution)/shard_map/reduce-window
  131.7 2.6 copy.29
  134.4 4.6 %fusion.64 = bf16[256,2048]{0,1:T(8,128)(2,1)S(1)} fusion(f32[1,256,16,128]{1,3,2,0:T(8,128)} %copy.29, f32[256,2048]{0,1:T(8,128)} %get-tuple-element.181, f32[256]{0:T(256)S(1)} %bitcast.82, f32[256,16]{0,1:T(8,128)S(1)} %slice_bitcast_fusion.7, s32[256]{0:T(256)S(1)} %iota_add_fusion.4, s32[2048]{0:T(1024)S(1)} %iota_add_fusion.5), kind=kLoop, calls=%fused_computation.8.clone.1 | loop fusion | flops 12058624 | bytes 5269504 | tf_op jit(solution)/shard_map/while/body/convert_element_type | solution.py:94
  139.0 1.3 fusion.65
  140.3 4.6 %fusion.62 = (f32[256]{0:T(256)S(1)}, f32[256,2048]{0,1:T(8,128)S(1)}, f32[256,2048]{0,1:T(8,128)}) fusion(s32[256]{0:T(256)S(1)} %iota_add_fusion.4, s32[2048]{0:T(1024)S(1)} %iota_add_fusion.5, f32[]{:T(128)} %bitcast.72, bf16[256,1,64]{0,2,1:T(8,128)(2,1)S(1)} %get-tuple-element.219, bf16[16384,1,64]{0,2,1:T(8,128)(2,1)} %get-tuple-element.218, ...), kind=kOutput, calls=%fused_computation.31.clone.1 | convolution fusion | flops 73400064 | bytes 4499972 | tf_op jit(solution)/shard_map/while/body/qhd,khd->hqk/dot_general | solution.py:84
  144.9 5.0 %fusion.63 = f32[1,256,16,128]{1,2,3,0:T(8,128)S(1)} fusion(f32[1,256,16,128]{1,3,2,0:T(8,128)S(1)} %bitcast.76), kind=kOutput, calls=%fused_computation.16.clone.1 | output fusion | flops 66584576 | bytes 4194304 | tf_op jit(solution)/shard_map/reduce-window
  149.9 2.6 copy.29
  152.6 4.6 %fusion.64 = bf16[256,2048]{0,1:T(8,128)(2,1)S(1)} fusion(f32[1,256,16,128]{1,3,2,0:T(8,128)} %copy.29, f32[256,2048]{0,1:T(8,128)} %get-tuple-element.181, f32[256]{0:T(256)S(1)} %bitcast.82, f32[256,16]{0,1:T(8,128)S(1)} %slice_bitcast_fusion.7, s32[256]{0:T(256)S(1)} %iota_add_fusion.4, s32[2048]{0:T(1024)S(1)} %iota_add_fusion.5), kind=kLoop, calls=%fused_computation.8.clone.1 | loop fusion | flops 12058624 | bytes 5269504 | tf_op jit(solution)/shard_map/while/body/convert_element_type | solution.py:94
  157.3 1.2 fusion.65
  158.6 4.6 %fusion.62 = (f32[256]{0:T(256)S(1)}, f32[256,2048]{0,1:T(8,128)S(1)}, f32[256,2048]{0,1:T(8,128)}) fusion(s32[256]{0:T(256)S(1)} %iota_add_fusion.4, s32[2048]{0:T(1024)S(1)} %iota_add_fusion.5, f32[]{:T(128)} %bitcast.72, bf16[256,1,64]{0,2,1:T(8,128)(2,1)S(1)} %get-tuple-element.219, bf16[16384,1,64]{0,2,1:T(8,128)(2,1)} %get-tuple-element.218, ...), kind=kOutput, calls=%fused_computation.31.clone.1 | convolution fusion | flops 73400064 | bytes 4499972 | tf_op jit(solution)/shard_map/while/body/qhd,khd->hqk/dot_general | solution.py:84
  163.1 5.0 %fusion.63 = f32[1,256,16,128]{1,2,3,0:T(8,128)S(1)} fusion(f32[1,256,16,128]{1,3,2,0:T(8,128)S(1)} %bitcast.76), kind=kOutput, calls=%fused_computation.16.clone.1 | output fusion | flops 66584576 | bytes 4194304 | tf_op jit(solution)/shard_map/reduce-window
  168.2 2.6 copy.29
  170.9 4.7 %fusion.64 = bf16[256,2048]{0,1:T(8,128)(2,1)S(1)} fusion(f32[1,256,16,128]{1,3,2,0:T(8,128)} %copy.29, f32[256,2048]{0,1:T(8,128)} %get-tuple-element.181, f32[256]{0:T(256)S(1)} %bitcast.82, f32[256,16]{0,1:T(8,128)S(1)} %slice_bitcast_fusion.7, s32[256]{0:T(256)S(1)} %iota_add_fusion.4, s32[2048]{0:T(1024)S(1)} %iota_add_fusion.5), kind=kLoop, calls=%fused_computation.8.clone.1 | loop fusion | flops 12058624 | bytes 5269504 | tf_op jit(solution)/shard_map/while/body/convert_element_type | solution.py:94
  175.6 1.3 fusion.65
  176.9 4.6 %fusion.62 = (f32[256]{0:T(256)S(1)}, f32[256,2048]{0,1:T(8,128)S(1)}, f32[256,2048]{0,1:T(8,128)}) fusion(s32[256]{0:T(256)S(1)} %iota_add_fusion.4, s32[2048]{0:T(1024)S(1)} %iota_add_fusion.5, f32[]{:T(128)} %bitcast.72, bf16[256,1,64]{0,2,1:T(8,128)(2,1)S(1)} %get-tuple-element.219, bf16[16384,1,64]{0,2,1:T(8,128)(2,1)} %get-tuple-element.218, ...), kind=kOutput, calls=%fused_computation.31.clone.1 | convolution fusion | flops 73400064 | bytes 4499972 | tf_op jit(solution)/shard_map/while/body/qhd,khd->hqk/dot_general | solution.py:84
  181.5 5.0 %fusion.63 = f32[1,256,16,128]{1,2,3,0:T(8,128)S(1)} fusion(f32[1,256,16,128]{1,3,2,0:T(8,128)S(1)} %bitcast.76), kind=kOutput, calls=%fused_computation.16.clone.1 | output fusion | flops 66584576 | bytes 4194304 | tf_op jit(solution)/shard_map/reduce-window
  186.5 2.6 copy.29
  189.2 4.6 %fusion.64 = bf16[256,2048]{0,1:T(8,128)(2,1)S(1)} fusion(f32[1,256,16,128]{1,3,2,0:T(8,128)} %copy.29, f32[256,2048]{0,1:T(8,128)} %get-tuple-element.181, f32[256]{0:T(256)S(1)} %bitcast.82, f32[256,16]{0,1:T(8,128)S(1)} %slice_bitcast_fusion.7, s32[256]{0:T(256)S(1)} %iota_add_fusion.4, s32[2048]{0:T(1024)S(1)} %iota_add_fusion.5), kind=kLoop, calls=%fused_computation.8.clone.1 | loop fusion | flops 12058624 | bytes 5269504 | tf_op jit(solution)/shard_map/while/body/convert_element_type | solution.py:94
  193.8 1.2 fusion.65
  195.1 4.5 %fusion.62 = (f32[256]{0:T(256)S(1)}, f32[256,2048]{0,1:T(8,128)S(1)}, f32[256,2048]{0,1:T(8,128)}) fusion(s32[256]{0:T(256)S(1)} %iota_add_fusion.4, s32[2048]{0:T(1024)S(1)} %iota_add_fusion.5, f32[]{:T(128)} %bitcast.72, bf16[256,1,64]{0,2,1:T(8,128)(2,1)S(1)} %get-tuple-element.219, bf16[16384,1,64]{0,2,1:T(8,128)(2,1)} %get-tuple-element.218, ...), kind=kOutput, calls=%fused_computation.31.clone.1 | convolution fusion | flops 73400064 | bytes 4499972 | tf_op jit(solution)/shard_map/while/body/qhd,khd->hqk/dot_general | solution.py:84
  199.7 5.0 %fusion.63 = f32[1,256,16,128]{1,2,3,0:T(8,128)S(1)} fusion(f32[1,256,16,128]{1,3,2,0:T(8,128)S(1)} %bitcast.76), kind=kOutput, calls=%fused_computation.16.clone.1 | output fusion | flops 66584576 | bytes 4194304 | tf_op jit(solution)/shard_map/reduce-window
  204.8 2.6 copy.29
  207.4 4.6 %fusion.64 = bf16[256,2048]{0,1:T(8,128)(2,1)S(1)} fusion(f32[1,256,16,128]{1,3,2,0:T(8,128)} %copy.29, f32[256,2048]{0,1:T(8,128)} %get-tuple-element.181, f32[256]{0:T(256)S(1)} %bitcast.82, f32[256,16]{0,1:T(8,128)S(1)} %slice_bitcast_fusion.7, s32[256]{0:T(256)S(1)} %iota_add_fusion.4, s32[2048]{0:T(1024)S(1)} %iota_add_fusion.5), kind=kLoop, calls=%fused_computation.8.clone.1 | loop fusion | flops 12058624 | bytes 5269504 | tf_op jit(solution)/shard_map/while/body/convert_element_type | solution.py:94
  212.1 1.2 fusion.65
  213.4 4.6 %fusion.62 = (f32[256]{0:T(256)S(1)}, f32[256,2048]{0,1:T(8,128)S(1)}, f32[256,2048]{0,1:T(8,128)}) fusion(s32[256]{0:T(256)S(1)} %iota_add_fusion.4, s32[2048]{0:T(1024)S(1)} %iota_add_fusion.5, f32[]{:T(128)} %bitcast.72, bf16[256,1,64]{0,2,1:T(8,128)(2,1)S(1)} %get-tuple-element.219, bf16[16384,1,64]{0,2,1:T(8,128)(2,1)} %get-tuple-element.218, ...), kind=kOutput, calls=%fused_computation.31.clone.1 | convolution fusion | flops 73400064 | bytes 4499972 | tf_op jit(solution)/shard_map/while/body/qhd,khd->hqk/dot_general | solution.py:84
  217.9 5.0 %fusion.63 = f32[1,256,16,128]{1,2,3,0:T(8,128)S(1)} fusion(f32[1,256,16,128]{1,3,2,0:T(8,128)S(1)} %bitcast.76), kind=kOutput, calls=%fused_computation.16.clone.1 | output fusion | flops 66584576 | bytes 4194304 | tf_op jit(solution)/shard_map/reduce-window
  223.0 2.6 copy.29
  225.7 4.6 %fusion.64 = bf16[256,2048]{0,1:T(8,128)(2,1)S(1)} fusion(f32[1,256,16,128]{1,3,2,0:T(8,128)} %copy.29, f32[256,2048]{0,1:T(8,128)} %get-tuple-element.181, f32[256]{0:T(256)S(1)} %bitcast.82, f32[256,16]{0,1:T(8,128)S(1)} %slice_bitcast_fusion.7, s32[256]{0:T(256)S(1)} %iota_add_fusion.4, s32[2048]{0:T(1024)S(1)} %iota_add_fusion.5), kind=kLoop, calls=%fused_computation.8.clone.1 | loop fusion | flops 12058624 | bytes 5269504 | tf_op jit(solution)/shard_map/while/body/convert_element_type | solution.py:94
  230.3 1.2 fusion.65
  231.6 4.6 %fusion.62 = (f32[256]{0:T(256)S(1)}, f32[256,2048]{0,1:T(8,128)S(1)}, f32[256,2048]{0,1:T(8,128)}) fusion(s32[256]{0:T(256)S(1)} %iota_add_fusion.4, s32[2048]{0:T(1024)S(1)} %iota_add_fusion.5, f32[]{:T(128)} %bitcast.72, bf16[256,1,64]{0,2,1:T(8,128)(2,1)S(1)} %get-tuple-element.219, bf16[16384,1,64]{0,2,1:T(8,128)(2,1)} %get-tuple-element.218, ...), kind=kOutput, calls=%fused_computation.31.clone.1 | convolution fusion | flops 73400064 | bytes 4499972 | tf_op jit(solution)/shard_map/while/body/qhd,khd->hqk/dot_general | solution.py:84
  236.2 5.0 %fusion.63 = f32[1,256,16,128]{1,2,3,0:T(8,128)S(1)} fusion(f32[1,256,16,128]{1,3,2,0:T(8,128)S(1)} %bitcast.76), kind=kOutput, calls=%fused_computation.16.clone.1 | output fusion | flops 66584576 | bytes 4194304 | tf_op jit(solution)/shard_map/reduce-window
  241.2 2.6 copy.29
  243.9 4.6 %fusion.64 = bf16[256,2048]{0,1:T(8,128)(2,1)S(1)} fusion(f32[1,256,16,128]{1,3,2,0:T(8,128)} %copy.29, f32[256,2048]{0,1:T(8,128)} %get-tuple-element.181, f32[256]{0:T(256)S(1)} %bitcast.82, f32[256,16]{0,1:T(8,128)S(1)} %slice_bitcast_fusion.7, s32[256]{0:T(256)S(1)} %iota_add_fusion.4, s32[2048]{0:T(1024)S(1)} %iota_add_fusion.5), kind=kLoop, calls=%fused_computation.8.clone.1 | loop fusion | flops 12058624 | bytes 5269504 | tf_op jit(solution)/shard_map/while/body/convert_element_type | solution.py:94
  248.6 1.3 fusion.65
  250.1 9.5 %all_to_all.26 = bf16[8,2,1024]{2,1,0:T(2,128)(2,1)S(1)} all-to-all(bf16[8,2,1024]{2,1,0:T(2,128)(2,1)S(1)} %reshape.137), channel_id=1, replica_groups=mesh['sp'=64,'tp'=8] {'tp'}, dimensions={0} | all-to-all | bytes 65536 | tf_op jit(solution)/shard_map/all_to_all | solution.py:127
  259.9 0.6 multiply_reduce_fusion
  260.5 0.2 fusion.40
  260.8 0.6 copy-done.1
  261.6 18.4 %all_to_all.27 = bf16[8,32,2048]{2,1,0:T(8,128)(2,1)S(1)} all-to-all(bf16[8,32,2048]{2,1,0:T(8,128)(2,1)S(1)} %broadcast_in_dim.16), channel_id=1, replica_groups=mesh['sp'=64,'tp'=8] {'tp'}, dimensions={0} | all-to-all | bytes 2097152 | tf_op jit(solution)/shard_map/all_to_all | solution.py:25
  280.0 3.3 %fusion.29 = bf16[256,704]{0,1:T(8,128)(2,1)S(1)} fusion(bf16[256,2048]{1,0:T(8,128)(2,1)S(1)} %bitcast.77, bf16[2048,1408]{1,0:T(8,128)(2,1)} %all-gather.6.cloned.1.call-done), kind=kOutput, calls=%fused_computation.46 | convolution fusion | flops 738377728 | bytes 4554752 | tf_op jit(solution)/shard_map/dot_general | solution.py:134
  283.4 0.2 copy-done.9
  283.6 2.7 fusion.32
  286.3 0.2 pad_maximum_fusion
  286.5 2.9 collective-permute-start
  289.5 10.7 %collective-permute-done = bf16[2,1408]{0,1:T(8,128)(2,1)S(1)} collective-permute-done((bf16[2,1408]{0,1:T(8,128)(2,1)S(1)}, bf16[2,1408]{0,1:T(8,128)(2,1)S(1)}, u32[]{:S(2)}, u32[]{:S(2)}) %collective-permute-start) | collective-permute-done | bytes 5664 | tf_op jit(solution)/shard_map/ppermute | solution.py:35
  300.3 0.5 maximum_convert_fusion
  300.8 1.5 fusion.27
  302.3 2.9 convolution_convert_fusion
  305.3 18.5 %all_to_all.28 = bf16[8,32,2048]{2,1,0:T(8,128)(2,1)S(1)} all-to-all(bf16[8,32,2048]{2,1,0:T(8,128)(2,1)S(1)} %bitcast.79), channel_id=1, replica_groups=mesh['sp'=64,'tp'=8] {'tp'}, dimensions={0} | all-to-all | bytes 2097152 | tf_op jit(solution)/shard_map/all_to_all | solution.py:45
  323.8 0.1 reduce_sum.52
  324.0 0.1 fusion.38
  324.1 0.8 fusion.43
  (88 shorter events, 1.7 us)
Async XLA Ops:
  6.5 253.4 %copy-start = (bf16[512,2048]{1,0:T(8,128)(2,1)S(1)}, bf16[512,2048]{1,0:T(8,128)(2,1)}, u32[]{:S(2)}) copy-start(bf16[512,2048]{1,0:T(8,128)(2,1)} %param.21) | copy-start | bytes 6291460
  6.5 92.7 %all-gather.4.cloned.1.call-start = ((), (), s32[]{:S(2)}) async-start(), calls=%async_computation.3 | async-start | bytes 4259840 | tf_op jit(solution)/shard_map/all_gather | solution.py:13
  8.1 271.9 %all-gather.6.cloned.1.call-start = ((), (), s32[]{:S(2)}) async-start(), calls=%async_computation.4 | async-start | bytes 5857280 | tf_op jit(solution)/shard_map/all_gather | solution.py:13
  9.7 292.6 %all-gather.8.cloned.1.call-start = ((), (), s32[]{:S(2)}) async-start(), calls=%async_computation.5 | async-start | bytes 3194880 | tf_op jit(solution)/shard_map/all_gather | solution.py:55
  10.5 93.3 %copy-start.10 = (bf16[256,64]{0,1:T(8,128)(2,1)S(1)}, bf16[256,64]{0,1:T(8,128)(2,1)}, u32[]{:S(2)}) copy-start(bf16[256,64]{0,1:T(8,128)(2,1)} %param.16) | copy-start | bytes 98308
  249.9 10.6 %copy-start.3 = (bf16[32,2048]{1,0:T(8,128)(2,1)S(1)}, bf16[32,2048]{1,0:T(8,128)(2,1)}, u32[]{:S(2)}) copy-start(bf16[32,2048]{1,0:T(8,128)(2,1)} %param.20) | copy-start | bytes 393220
  249.9 10.6 %copy-start.6 = (f32[2048]{0:T(1024)S(1)}, f32[2048]{0:T(1024)}, u32[]{:S(2)}) copy-start(f32[2048]{0:T(1024)} %param.22) | copy-start | bytes 24580
  249.9 11.5 %copy-start.7 = (f32[2048]{0:T(1024)S(1)}, f32[2048]{0:T(1024)}, u32[]{:S(2)}) copy-start(f32[2048]{0:T(1024)} %param.23) | copy-start | bytes 24580
  260.7 0.7 copy-start.1
  280.0 3.6 %copy-start.9 = (bf16[2048,1408]{1,0:T(8,128)(2,1)S(1)}, bf16[2048,1408]{1,0:T(8,128)(2,1)}, u32[]{:S(2)}) copy-start(bf16[2048,1408]{1,0:T(8,128)(2,1)} %all-gather.6.cloned.1.call-done) | copy-start | bytes 17301508
  283.6 5.8 %copy-start.4 = (f32[3,704]{1,0:T(4,128)S(1)}, f32[3,704]{1,0:T(4,128)}, u32[]{:S(2)}) copy-start(f32[3,704]{1,0:T(4,128)} %param.27) | copy-start | bytes 25348
  283.6 5.8 %copy-start.5 = (f32[3,704]{1,0:T(4,128)S(1)}, f32[3,704]{1,0:T(4,128)}, u32[]{:S(2)}) copy-start(f32[3,704]{1,0:T(4,128)} %param.26) | copy-start | bytes 25348
  286.5 13.8 %collective-permute-start = (bf16[2,1408]{0,1:T(8,128)(2,1)S(1)}, bf16[2,1408]{0,1:T(8,128)(2,1)S(1)}, u32[]{:S(2)}, u32[]{:S(2)}) collective-permute-start(bf16[2,1408]{0,1:T(8,128)(2,1)S(1)} %pad_maximum_fusion), channel_id=1, source_target_pairs={{0,8},{8,16},{16,24},{24,32},{32,40},{40,48},{48,56},{56,64},{64,7... | collective-permute-start | bytes 16904 | tf_op jit(solution)/shard_map/ppermute | solution.py:35
  305.3 18.9 %copy-start.2 = (bf16[32,2048]{1,0:T(8,128)(2,1)S(1)}, bf16[32,2048]{1,0:T(8,128)(2,1)}, u32[]{:S(2)}) copy-start(bf16[32,2048]{1,0:T(8,128)(2,1)} %copy-done.1) | copy-start | bytes 393220
  305.3 18.8 %copy-start.8 = (f32[2048]{0:T(1024)S(1)}, f32[2048]{0:T(1024)}, u32[]{:S(2)}) copy-start(f32[2048]{0:T(1024)} %param.29) | copy-start | bytes 24580
Sparse Core Ops, SparseCore 0:
  10.3 88.8 all-gather.3
  102.2 85.3 all-gather.5
  190.6 82.1 all-gather.7
where the time goes:
time: 332 us; the launch traced here: 331 us
  waiting for transfers between devices  100 us (30%)
  other arithmetic  84.9 us (26%)
  matrix products  56 us (17%)
  blocking collectives  46.4 us (14%)
  local copies, waits for them, and re-layouts  27 us (8%)
  between operations  13.3 us (4%)
    all_gather x2, waiting for transfers between devices, side_by_side(): out = lax.all_gather(both, axis, axis=dim, tiled=True)  88.7 us
    another operation x16, other arithmetic  40.8 us
    convert_element_type x8, other arithmetic, visit(): weights = jnp.where(causal, jnp.exp(jax.nn.log_sigmoid(scores) + later +...  37.1 us
    dot_general x8, matrix products, visit(): jnp.einsum('qhd,khd->hqk', query_heads, key_block, preferred_element_type...  36.4 us
    another operation x24, local copies, waits for them, and re-layouts  21 us
    all_to_all x1, blocking collectives, sum_at_owner(): lax.all_to_all(parts, axis, split_axis=0, concat_axis=0, tiled=True)  18.5 us
    all_to_all x1, blocking collectives, from_everyone(): lax.all_to_all(jnp.broadcast_to(x[None], (length, *x.shape)), axis, 0, 0,...  18.4 us
    ppermute x1, waiting for transfers between devices, from_behind(): return lax.ppermute(x, axis, pairs)  10.7 us
  transfers between devices with their start and end apart: 4, of which 2 were waited for; matrix products, arithmetic and copies ran while one was open for 49% of the time, Pallas kernels for 0%

commit v1 on v0

--- a/solution.py
+++ b/solution.py
@@ -2,6 +2,7 @@
 import jax.numpy as jnp
 from jax import lax
 from jax.sharding import PartitionSpec as P
+from jax.lax import all_to_all, axis_size
 
 HEAD_DIM = 64
 KERNEL = 3
@@ -124,7 +125,9 @@
     gate_whole, up_whole, down_whole = collect_weights(w_gate, w_up, w_down)
     key_whole, value_whole = side_by_side((keys, values), "sp", 0, 1)
     attended = stick_attention(queries, key_whole, value_whole, score_shift)
-    head_rows = lax.all_to_all(attended, "tp", split_axis=0, concat_axis=1, tiled=True)
+    head_rows = jnp.concatenate(
+        all_to_all(jnp.stack(jnp.split(attended, axis_size("tp"), axis=0)), "tp", 0, 0), axis=1
+    )
     mixed = jnp.dot(head_rows, w_out, preferred_element_type=jnp.float32).astype(jnp.bfloat16)
     middle = (resid.astype(jnp.float32) + gain_mix * rms_scale(mixed.astype(jnp.float32))).astype(
         jnp.bfloat16

time: 332 us -> 332 us (level)
    another operation x24 -> x25, local copies, waits for them, and re-layouts: 21 us -> 21 us
where the time goes in v1:
time: 332 us
  waiting for transfers between devices  100 us (30%)
  other arithmetic  84.9 us (26%)
  matrix products  56 us (17%)
  blocking collectives  46.4 us (14%)
  local copies, waits for them, and re-layouts  27.1 us (8%)
  between operations  13.4 us (4%)
    all_gather x2, waiting for transfers between devices, side_by_side(): out = lax.all_gather(both, axis, axis=dim, tiled=True)  88.7 us
    another operation x16, other arithmetic  40.8 us
    convert_element_type x8, other arithmetic, visit(): weights = jnp.where(causal, jnp.exp(jax.nn.log_sigmoid(scores) + later +...  37.1 us
    dot_general x8, matrix products, visit(): jnp.einsum('qhd,khd->hqk', query_heads, key_block, preferred_element_type...  36.4 us
    another operation x24, local copies, waits for them, and re-layouts  21 us
    all_to_all x1, blocking collectives, sum_at_owner(): lax.all_to_all(parts, axis, split_axis=0, concat_axis=0, tiled=True)  18.5 us
    all_to_all x1, blocking collectives, from_everyone(): lax.all_to_all(jnp.broadcast_to(x[None], (length, *x.shape)), axis, 0, 0,...  18.4 us
    ppermute x1, waiting for transfers between devices, from_behind(): return lax.ppermute(x, axis, pairs)  10.7 us
  transfers between devices with their start and end apart: 4, of which 2 were waited for; matrix products, arithmetic and copies ran while one was open for 49% of the time, Pallas kernels for 0%

profile of v1, /device:TPU:448, one launch (start us, length us, event | category | flops | bytes accessed | tf_op | source)
XLA Modules:
  0.0 331.5 jit_solution(5135130780065827146)
XLA Ops:
  6.5 1.6 pad_maximum_fusion.2
  8.2 1.5 pad_maximum_fusion.1
  9.8 0.7 all-gather.8.cloned.1.call-update
  10.5 88.7 %all-gather.4.cloned.1.call-done = bf16[16384,128]{0,1:T(8,128)(2,1)} async-done(((bf16[256,128]{0,1:T(8,128)(2,1)}), bf16[16384,128]{0,1:T(8,128)(2,1)}) %all-gather.4.cloned.1.call-update) | async-done | bytes 4194320 | tf_op jit(solution)/shard_map/all_gather | solution.py:14
  99.2 4.5 %slice_bitcast_fusion.2 = (bf16[16384,1,64]{0,2,1:T(8,128)(2,1)}, bf16[16384,1,64]{0,2,1:T(8,128)(2,1)}) fusion(bf16[16384,128]{0,1:T(8,128)(2,1)} %all-gather.4.cloned.1.call-done), kind=kLoop, calls=%fused_computation.39 | loop fusion | bytes 8388608 | tf_op jit(solution)/shard_map/reshape | solution.py:76
  103.8 146.1 %while.13 = (s32[]{:T(128)}, f32[1,256,64]{1,2,0:T(8,128)S(1)}, f32[1,256]{1,0:T(1,128)S(1)}, s32[]{:T(128)}, s32[]{:T(128)}, /*index=5*/bf16[16384,1,64]{0,2,1:...) while((s32[]{:T(128)}, f32[1,256,64]{1,2,0:T(8,128)S(1)}, ...), condition=%wide.region_4.5_spmd.clone, body=%wide.region_0.4_spmd.clone.sunk | while | flops 219236352 | bytes 19711708 | solution.py:105
  103.8 4.6 %fusion.62 = (f32[256]{0:T(256)S(1)}, f32[256,2048]{0,1:T(8,128)S(1)}, f32[256,2048]{0,1:T(8,128)}) fusion(s32[256]{0:T(256)S(1)} %iota_add_fusion.4, s32[2048]{0:T(1024)S(1)} %iota_add_fusion.5, f32[]{:T(128)} %bitcast.71, bf16[256,1,64]{0,2,1:T(8,128)(2,1)S(1)} %get-tuple-element.219, bf16[16384,1,64]{0,2,1:T(8,128)(2,1)} %get-tuple-element.218, ...), kind=kOutput, calls=%fused_computation.31.clone.1 | convolution fusion | flops 73400064 | bytes 4499972 | tf_op jit(solution)/shard_map/while/body/qhd,khd->hqk/dot_general | solution.py:85
  108.4 5.0 %fusion.63 = f32[1,256,16,128]{1,2,3,0:T(8,128)S(1)} fusion(f32[1,256,16,128]{1,3,2,0:T(8,128)S(1)} %bitcast.75), kind=kOutput, calls=%fused_computation.16.clone.1 | output fusion | flops 66584576 | bytes 4194304 | tf_op jit(solution)/shard_map/reduce-window
  113.4 2.6 copy.34
  116.1 4.6 %fusion.64 = bf16[256,2048]{0,1:T(8,128)(2,1)S(1)} fusion(f32[1,256,16,128]{1,3,2,0:T(8,128)} %copy.34, f32[256,2048]{0,1:T(8,128)} %get-tuple-element.181, f32[256]{0:T(256)S(1)} %bitcast.80, f32[256,16]{0,1:T(8,128)S(1)} %slice_bitcast_fusion.7, s32[256]{0:T(256)S(1)} %iota_add_fusion.4, s32[2048]{0:T(1024)S(1)} %iota_add_fusion.5), kind=kLoop, calls=%fused_computation.8.clone.1 | loop fusion | flops 12058624 | bytes 5269504 | tf_op jit(solution)/shard_map/while/body/convert_element_type | solution.py:95
  120.8 1.3 fusion.65
  122.1 4.6 %fusion.62 = (f32[256]{0:T(256)S(1)}, f32[256,2048]{0,1:T(8,128)S(1)}, f32[256,2048]{0,1:T(8,128)}) fusion(s32[256]{0:T(256)S(1)} %iota_add_fusion.4, s32[2048]{0:T(1024)S(1)} %iota_add_fusion.5, f32[]{:T(128)} %bitcast.71, bf16[256,1,64]{0,2,1:T(8,128)(2,1)S(1)} %get-tuple-element.219, bf16[16384,1,64]{0,2,1:T(8,128)(2,1)} %get-tuple-element.218, ...), kind=kOutput, calls=%fused_computation.31.clone.1 | convolution fusion | flops 73400064 | bytes 4499972 | tf_op jit(solution)/shard_map/while/body/qhd,khd->hqk/dot_general | solution.py:85
  126.6 5.0 %fusion.63 = f32[1,256,16,128]{1,2,3,0:T(8,128)S(1)} fusion(f32[1,256,16,128]{1,3,2,0:T(8,128)S(1)} %bitcast.75), kind=kOutput, calls=%fused_computation.16.clone.1 | output fusion | flops 66584576 | bytes 4194304 | tf_op jit(solution)/shard_map/reduce-window
  131.7 2.6 copy.34
  134.4 4.6 %fusion.64 = bf16[256,2048]{0,1:T(8,128)(2,1)S(1)} fusion(f32[1,256,16,128]{1,3,2,0:T(8,128)} %copy.34, f32[256,2048]{0,1:T(8,128)} %get-tuple-element.181, f32[256]{0:T(256)S(1)} %bitcast.80, f32[256,16]{0,1:T(8,128)S(1)} %slice_bitcast_fusion.7, s32[256]{0:T(256)S(1)} %iota_add_fusion.4, s32[2048]{0:T(1024)S(1)} %iota_add_fusion.5), kind=kLoop, calls=%fused_computation.8.clone.1 | loop fusion | flops 12058624 | bytes 5269504 | tf_op jit(solution)/shard_map/while/body/convert_element_type | solution.py:95
  139.0 1.3 fusion.65
  140.3 4.6 %fusion.62 = (f32[256]{0:T(256)S(1)}, f32[256,2048]{0,1:T(8,128)S(1)}, f32[256,2048]{0,1:T(8,128)}) fusion(s32[256]{0:T(256)S(1)} %iota_add_fusion.4, s32[2048]{0:T(1024)S(1)} %iota_add_fusion.5, f32[]{:T(128)} %bitcast.71, bf16[256,1,64]{0,2,1:T(8,128)(2,1)S(1)} %get-tuple-element.219, bf16[16384,1,64]{0,2,1:T(8,128)(2,1)} %get-tuple-element.218, ...), kind=kOutput, calls=%fused_computation.31.clone.1 | convolution fusion | flops 73400064 | bytes 4499972 | tf_op jit(solution)/shard_map/while/body/qhd,khd->hqk/dot_general | solution.py:85
  144.9 5.0 %fusion.63 = f32[1,256,16,128]{1,2,3,0:T(8,128)S(1)} fusion(f32[1,256,16,128]{1,3,2,0:T(8,128)S(1)} %bitcast.75), kind=kOutput, calls=%fused_computation.16.clone.1 | output fusion | flops 66584576 | bytes 4194304 | tf_op jit(solution)/shard_map/reduce-window
  149.9 2.6 copy.34
  152.6 4.6 %fusion.64 = bf16[256,2048]{0,1:T(8,128)(2,1)S(1)} fusion(f32[1,256,16,128]{1,3,2,0:T(8,128)} %copy.34, f32[256,2048]{0,1:T(8,128)} %get-tuple-element.181, f32[256]{0:T(256)S(1)} %bitcast.80, f32[256,16]{0,1:T(8,128)S(1)} %slice_bitcast_fusion.7, s32[256]{0:T(256)S(1)} %iota_add_fusion.4, s32[2048]{0:T(1024)S(1)} %iota_add_fusion.5), kind=kLoop, calls=%fused_computation.8.clone.1 | loop fusion | flops 12058624 | bytes 5269504 | tf_op jit(solution)/shard_map/while/body/convert_element_type | solution.py:95
  157.3 1.2 fusion.65
  158.6 4.6 %fusion.62 = (f32[256]{0:T(256)S(1)}, f32[256,2048]{0,1:T(8,128)S(1)}, f32[256,2048]{0,1:T(8,128)}) fusion(s32[256]{0:T(256)S(1)} %iota_add_fusion.4, s32[2048]{0:T(1024)S(1)} %iota_add_fusion.5, f32[]{:T(128)} %bitcast.71, bf16[256,1,64]{0,2,1:T(8,128)(2,1)S(1)} %get-tuple-element.219, bf16[16384,1,64]{0,2,1:T(8,128)(2,1)} %get-tuple-element.218, ...), kind=kOutput, calls=%fused_computation.31.clone.1 | convolution fusion | flops 73400064 | bytes 4499972 | tf_op jit(solution)/shard_map/while/body/qhd,khd->hqk/dot_general | solution.py:85
  163.1 5.0 %fusion.63 = f32[1,256,16,128]{1,2,3,0:T(8,128)S(1)} fusion(f32[1,256,16,128]{1,3,2,0:T(8,128)S(1)} %bitcast.75), kind=kOutput, calls=%fused_computation.16.clone.1 | output fusion | flops 66584576 | bytes 4194304 | tf_op jit(solution)/shard_map/reduce-window
  168.2 2.6 copy.34
  170.9 4.7 %fusion.64 = bf16[256,2048]{0,1:T(8,128)(2,1)S(1)} fusion(f32[1,256,16,128]{1,3,2,0:T(8,128)} %copy.34, f32[256,2048]{0,1:T(8,128)} %get-tuple-element.181, f32[256]{0:T(256)S(1)} %bitcast.80, f32[256,16]{0,1:T(8,128)S(1)} %slice_bitcast_fusion.7, s32[256]{0:T(256)S(1)} %iota_add_fusion.4, s32[2048]{0:T(1024)S(1)} %iota_add_fusion.5), kind=kLoop, calls=%fused_computation.8.clone.1 | loop fusion | flops 12058624 | bytes 5269504 | tf_op jit(solution)/shard_map/while/body/convert_element_type | solution.py:95
  175.6 1.3 fusion.65
  176.9 4.6 %fusion.62 = (f32[256]{0:T(256)S(1)}, f32[256,2048]{0,1:T(8,128)S(1)}, f32[256,2048]{0,1:T(8,128)}) fusion(s32[256]{0:T(256)S(1)} %iota_add_fusion.4, s32[2048]{0:T(1024)S(1)} %iota_add_fusion.5, f32[]{:T(128)} %bitcast.71, bf16[256,1,64]{0,2,1:T(8,128)(2,1)S(1)} %get-tuple-element.219, bf16[16384,1,64]{0,2,1:T(8,128)(2,1)} %get-tuple-element.218, ...), kind=kOutput, calls=%fused_computation.31.clone.1 | convolution fusion | flops 73400064 | bytes 4499972 | tf_op jit(solution)/shard_map/while/body/qhd,khd->hqk/dot_general | solution.py:85
  181.5 5.0 %fusion.63 = f32[1,256,16,128]{1,2,3,0:T(8,128)S(1)} fusion(f32[1,256,16,128]{1,3,2,0:T(8,128)S(1)} %bitcast.75), kind=kOutput, calls=%fused_computation.16.clone.1 | output fusion | flops 66584576 | bytes 4194304 | tf_op jit(solution)/shard_map/reduce-window
  186.5 2.6 copy.34
  189.2 4.6 %fusion.64 = bf16[256,2048]{0,1:T(8,128)(2,1)S(1)} fusion(f32[1,256,16,128]{1,3,2,0:T(8,128)} %copy.34, f32[256,2048]{0,1:T(8,128)} %get-tuple-element.181, f32[256]{0:T(256)S(1)} %bitcast.80, f32[256,16]{0,1:T(8,128)S(1)} %slice_bitcast_fusion.7, s32[256]{0:T(256)S(1)} %iota_add_fusion.4, s32[2048]{0:T(1024)S(1)} %iota_add_fusion.5), kind=kLoop, calls=%fused_computation.8.clone.1 | loop fusion | flops 12058624 | bytes 5269504 | tf_op jit(solution)/shard_map/while/body/convert_element_type | solution.py:95
  193.8 1.2 fusion.65
  195.1 4.5 %fusion.62 = (f32[256]{0:T(256)S(1)}, f32[256,2048]{0,1:T(8,128)S(1)}, f32[256,2048]{0,1:T(8,128)}) fusion(s32[256]{0:T(256)S(1)} %iota_add_fusion.4, s32[2048]{0:T(1024)S(1)} %iota_add_fusion.5, f32[]{:T(128)} %bitcast.71, bf16[256,1,64]{0,2,1:T(8,128)(2,1)S(1)} %get-tuple-element.219, bf16[16384,1,64]{0,2,1:T(8,128)(2,1)} %get-tuple-element.218, ...), kind=kOutput, calls=%fused_computation.31.clone.1 | convolution fusion | flops 73400064 | bytes 4499972 | tf_op jit(solution)/shard_map/while/body/qhd,khd->hqk/dot_general | solution.py:85
  199.7 5.0 %fusion.63 = f32[1,256,16,128]{1,2,3,0:T(8,128)S(1)} fusion(f32[1,256,16,128]{1,3,2,0:T(8,128)S(1)} %bitcast.75), kind=kOutput, calls=%fused_computation.16.clone.1 | output fusion | flops 66584576 | bytes 4194304 | tf_op jit(solution)/shard_map/reduce-window
  204.8 2.6 copy.34
  207.4 4.6 %fusion.64 = bf16[256,2048]{0,1:T(8,128)(2,1)S(1)} fusion(f32[1,256,16,128]{1,3,2,0:T(8,128)} %copy.34, f32[256,2048]{0,1:T(8,128)} %get-tuple-element.181, f32[256]{0:T(256)S(1)} %bitcast.80, f32[256,16]{0,1:T(8,128)S(1)} %slice_bitcast_fusion.7, s32[256]{0:T(256)S(1)} %iota_add_fusion.4, s32[2048]{0:T(1024)S(1)} %iota_add_fusion.5), kind=kLoop, calls=%fused_computation.8.clone.1 | loop fusion | flops 12058624 | bytes 5269504 | tf_op jit(solution)/shard_map/while/body/convert_element_type | solution.py:95
  212.1 1.2 fusion.65
  213.4 4.6 %fusion.62 = (f32[256]{0:T(256)S(1)}, f32[256,2048]{0,1:T(8,128)S(1)}, f32[256,2048]{0,1:T(8,128)}) fusion(s32[256]{0:T(256)S(1)} %iota_add_fusion.4, s32[2048]{0:T(1024)S(1)} %iota_add_fusion.5, f32[]{:T(128)} %bitcast.71, bf16[256,1,64]{0,2,1:T(8,128)(2,1)S(1)} %get-tuple-element.219, bf16[16384,1,64]{0,2,1:T(8,128)(2,1)} %get-tuple-element.218, ...), kind=kOutput, calls=%fused_computation.31.clone.1 | convolution fusion | flops 73400064 | bytes 4499972 | tf_op jit(solution)/shard_map/while/body/qhd,khd->hqk/dot_general | solution.py:85
  217.9 5.0 %fusion.63 = f32[1,256,16,128]{1,2,3,0:T(8,128)S(1)} fusion(f32[1,256,16,128]{1,3,2,0:T(8,128)S(1)} %bitcast.75), kind=kOutput, calls=%fused_computation.16.clone.1 | output fusion | flops 66584576 | bytes 4194304 | tf_op jit(solution)/shard_map/reduce-window
  223.0 2.6 copy.34
  225.7 4.6 %fusion.64 = bf16[256,2048]{0,1:T(8,128)(2,1)S(1)} fusion(f32[1,256,16,128]{1,3,2,0:T(8,128)} %copy.34, f32[256,2048]{0,1:T(8,128)} %get-tuple-element.181, f32[256]{0:T(256)S(1)} %bitcast.80, f32[256,16]{0,1:T(8,128)S(1)} %slice_bitcast_fusion.7, s32[256]{0:T(256)S(1)} %iota_add_fusion.4, s32[2048]{0:T(1024)S(1)} %iota_add_fusion.5), kind=kLoop, calls=%fused_computation.8.clone.1 | loop fusion | flops 12058624 | bytes 5269504 | tf_op jit(solution)/shard_map/while/body/convert_element_type | solution.py:95
  230.3 1.2 fusion.65
  231.6 4.6 %fusion.62 = (f32[256]{0:T(256)S(1)}, f32[256,2048]{0,1:T(8,128)S(1)}, f32[256,2048]{0,1:T(8,128)}) fusion(s32[256]{0:T(256)S(1)} %iota_add_fusion.4, s32[2048]{0:T(1024)S(1)} %iota_add_fusion.5, f32[]{:T(128)} %bitcast.71, bf16[256,1,64]{0,2,1:T(8,128)(2,1)S(1)} %get-tuple-element.219, bf16[16384,1,64]{0,2,1:T(8,128)(2,1)} %get-tuple-element.218, ...), kind=kOutput, calls=%fused_computation.31.clone.1 | convolution fusion | flops 73400064 | bytes 4499972 | tf_op jit(solution)/shard_map/while/body/qhd,khd->hqk/dot_general | solution.py:85
  236.2 5.0 %fusion.63 = f32[1,256,16,128]{1,2,3,0:T(8,128)S(1)} fusion(f32[1,256,16,128]{1,3,2,0:T(8,128)S(1)} %bitcast.75), kind=kOutput, calls=%fused_computation.16.clone.1 | output fusion | flops 66584576 | bytes 4194304 | tf_op jit(solution)/shard_map/reduce-window
  241.2 2.6 copy.34
  243.9 4.6 %fusion.64 = bf16[256,2048]{0,1:T(8,128)(2,1)S(1)} fusion(f32[1,256,16,128]{1,3,2,0:T(8,128)} %copy.34, f32[256,2048]{0,1:T(8,128)} %get-tuple-element.181, f32[256]{0:T(256)S(1)} %bitcast.80, f32[256,16]{0,1:T(8,128)S(1)} %slice_bitcast_fusion.7, s32[256]{0:T(256)S(1)} %iota_add_fusion.4, s32[2048]{0:T(1024)S(1)} %iota_add_fusion.5), kind=kLoop, calls=%fused_computation.8.clone.1 | loop fusion | flops 12058624 | bytes 5269504 | tf_op jit(solution)/shard_map/while/body/convert_element_type | solution.py:95
  248.6 1.3 fusion.65
  250.2 9.5 %all_to_all.15 = bf16[8,2,1024]{2,1,0:T(2,128)(2,1)S(1)} all-to-all(bf16[8,2,1024]{2,1,0:T(2,128)(2,1)S(1)} %reshape.157), channel_id=1, replica_groups=mesh['sp'=64,'tp'=8] {'tp'}, dimensions={0} | all-to-all | bytes 65536 | tf_op jit(solution)/shard_map/all_to_all | solution.py:129
  260.0 0.6 multiply_reduce_fusion
  260.6 0.2 fusion.40
  260.8 0.6 copy-done.1
  261.7 18.4 %all_to_all.16 = bf16[8,32,2048]{2,1,0:T(8,128)(2,1)S(1)} all-to-all(bf16[8,32,2048]{2,1,0:T(8,128)(2,1)S(1)} %broadcast_in_dim.16), channel_id=1, replica_groups=mesh['sp'=64,'tp'=8] {'tp'}, dimensions={0} | all-to-all | bytes 2097152 | tf_op jit(solution)/shard_map/all_to_all | solution.py:26
  280.1 3.3 %fusion.29 = bf16[256,704]{0,1:T(8,128)(2,1)S(1)} fusion(bf16[256,2048]{1,0:T(8,128)(2,1)S(1)} %bitcast.76, bf16[2048,1408]{1,0:T(8,128)(2,1)} %all-gather.6.cloned.1.call-done), kind=kOutput, calls=%fused_computation.46 | convolution fusion | flops 738377728 | bytes 4554752 | tf_op jit(solution)/shard_map/dot_general | solution.py:137
  283.4 0.2 copy-done.9
  283.7 2.7 fusion.32
  286.4 0.2 pad_maximum_fusion
  286.6 2.9 collective-permute-start
  289.6 10.7 %collective-permute-done = bf16[2,1408]{0,1:T(8,128)(2,1)S(1)} collective-permute-done((bf16[2,1408]{0,1:T(8,128)(2,1)S(1)}, bf16[2,1408]{0,1:T(8,128)(2,1)S(1)}, u32[]{:S(2)}, u32[]{:S(2)}) %collective-permute-start) | collective-permute-done | bytes 5664 | tf_op jit(solution)/shard_map/ppermute | solution.py:36
  300.3 0.5 maximum_convert_fusion
  300.8 1.5 fusion.27
  302.4 2.9 convolution_convert_fusion
  305.4 18.5 %all_to_all.17 = bf16[8,32,2048]{2,1,0:T(8,128)(2,1)S(1)} all-to-all(bf16[8,32,2048]{2,1,0:T(8,128)(2,1)S(1)} %bitcast.78), channel_id=1, replica_groups=mesh['sp'=64,'tp'=8] {'tp'}, dimensions={0} | all-to-all | bytes 2097152 | tf_op jit(solution)/shard_map/all_to_all | solution.py:46
  323.9 0.1 reduce_sum.52
  324.0 0.1 fusion.38
  324.2 0.8 fusion.43
  (96 shorter events, 1.8 us)
Async XLA Ops:
  6.5 253.4 %copy-start = (bf16[512,2048]{1,0:T(8,128)(2,1)S(1)}, bf16[512,2048]{1,0:T(8,128)(2,1)}, u32[]{:S(2)}) copy-start(bf16[512,2048]{1,0:T(8,128)(2,1)} %param.21) | copy-start | bytes 6291460
  6.5 92.7 %all-gather.4.cloned.1.call-start = ((), (), s32[]{:S(2)}) async-start(), calls=%async_computation.3 | async-start | bytes 4259840 | tf_op jit(solution)/shard_map/all_gather | solution.py:14
  8.1 272.0 %all-gather.6.cloned.1.call-start = ((), (), s32[]{:S(2)}) async-start(), calls=%async_computation.4 | async-start | bytes 5857280 | tf_op jit(solution)/shard_map/all_gather | solution.py:14
  9.7 292.6 %all-gather.8.cloned.1.call-start = ((), (), s32[]{:S(2)}) async-start(), calls=%async_computation.5 | async-start | bytes 3194880 | tf_op jit(solution)/shard_map/all_gather | solution.py:56
  10.5 93.3 %copy-start.10 = (bf16[256,64]{0,1:T(8,128)(2,1)S(1)}, bf16[256,64]{0,1:T(8,128)(2,1)}, u32[]{:S(2)}) copy-start(bf16[256,64]{0,1:T(8,128)(2,1)} %param.16) | copy-start | bytes 98308
  249.9 10.7 %copy-start.3 = (bf16[32,2048]{1,0:T(8,128)(2,1)S(1)}, bf16[32,2048]{1,0:T(8,128)(2,1)}, u32[]{:S(2)}) copy-start(bf16[32,2048]{1,0:T(8,128)(2,1)} %param.20) | copy-start | bytes 393220
  249.9 10.7 %copy-start.6 = (f32[2048]{0:T(1024)S(1)}, f32[2048]{0:T(1024)}, u32[]{:S(2)}) copy-start(f32[2048]{0:T(1024)} %param.22) | copy-start | bytes 24580
  249.9 11.6 %copy-start.7 = (f32[2048]{0:T(1024)S(1)}, f32[2048]{0:T(1024)}, u32[]{:S(2)}) copy-start(f32[2048]{0:T(1024)} %param.23) | copy-start | bytes 24580
  260.8 0.7 copy-start.1
  280.1 3.6 %copy-start.9 = (bf16[2048,1408]{1,0:T(8,128)(2,1)S(1)}, bf16[2048,1408]{1,0:T(8,128)(2,1)}, u32[]{:S(2)}) copy-start(bf16[2048,1408]{1,0:T(8,128)(2,1)} %all-gather.6.cloned.1.call-done) | copy-start | bytes 17301508
  283.7 5.8 %copy-start.4 = (f32[3,704]{1,0:T(4,128)S(1)}, f32[3,704]{1,0:T(4,128)}, u32[]{:S(2)}) copy-start(f32[3,704]{1,0:T(4,128)} %param.27) | copy-start | bytes 25348
  283.7 5.8 %copy-start.5 = (f32[3,704]{1,0:T(4,128)S(1)}, f32[3,704]{1,0:T(4,128)}, u32[]{:S(2)}) copy-start(f32[3,704]{1,0:T(4,128)} %param.26) | copy-start | bytes 25348
  286.6 13.8 %collective-permute-start = (bf16[2,1408]{0,1:T(8,128)(2,1)S(1)}, bf16[2,1408]{0,1:T(8,128)(2,1)S(1)}, u32[]{:S(2)}, u32[]{:S(2)}) collective-permute-start(bf16[2,1408]{0,1:T(8,128)(2,1)S(1)} %pad_maximum_fusion), channel_id=1, source_target_pairs={{0,8},{8,16},{16,24},{24,32},{32,40},{40,48},{48,56},{56,64},{64,7... | collective-permute-start | bytes 16904 | tf_op jit(solution)/shard_map/ppermute | solution.py:36
  305.3 18.9 %copy-start.2 = (bf16[32,2048]{1,0:T(8,128)(2,1)S(1)}, bf16[32,2048]{1,0:T(8,128)(2,1)}, u32[]{:S(2)}) copy-start(bf16[32,2048]{1,0:T(8,128)(2,1)} %copy-done.1) | copy-start | bytes 393220
  305.4 18.8 %copy-start.8 = (f32[2048]{0:T(1024)S(1)}, f32[2048]{0:T(1024)}, u32[]{:S(2)}) copy-start(f32[2048]{0:T(1024)} %param.29) | copy-start | bytes 24580
Sparse Core Ops, SparseCore 0:
  10.3 88.8 all-gather.3
  102.2 85.3 all-gather.5
  190.6 82.1 all-gather.7
